TPU v7x, 512 devices: a whole 4x8x8 slice. The times are simulated.
512 devices in a mesh: kv: 64 (over z, y), tp: 8 (over x, core).
Axes of the slice: x: 4, y: 8, z: 8, core: 2. Of those that a mesh axis runs over, the one named last changes fastest.
Arguments:
- tokens: bfloat16 [256, 4, 2048], P('kv', None, 'tp'), may hold values from -6 to 6
- input_gain: float32 [2048], replicated, may hold values from 0.1 to 1.9
- gate_weight: bfloat16 [2048, 4096], P('kv', 'tp'), may hold values from -0.125 to 0.125
- value_weight: bfloat16 [2048, 4096], P('kv', 'tp'), may hold values from -0.125 to 0.125
- write_weight: bfloat16 [2048, 1024], P('kv', 'tp'), may hold values from -0.125 to 0.125
- read_weight: bfloat16 [2048, 1024], P('kv', 'tp'), may hold values from -0.125 to 0.125
- step_weight: bfloat16 [2048, 64], replicated, may hold values from -0.125 to 0.125
- conv_value: float32 [4, 4096], P(None, 'tp'), may hold values from -3 to 3
- conv_write: float32 [4, 1024], P(None, 'tp'), may hold values from -3 to 3
- conv_read: float32 [4, 1024], P(None, 'tp'), may hold values from -3 to 3
- step_bias: float32 [64], P('tp'), may hold values from -4 to -1
- decay_log: float32 [64], P('tp'), may hold values from 0 to 2.8
- skip_gain: float32 [64], P('tp'), may hold values from 0.5 to 1.5
- output_gain: float32 [4096], P('tp'), may hold values from 0.1 to 1.9
- out_weight: bfloat16 [4096, 2048], P('tp', 'kv'), may hold values from -0.09375 to 0.09375
- base_state: float32 [256, 64, 64, 128], P('kv', 'tp'), may hold values from -2 to 2
- past_value: bfloat16 [256, 7, 4096], P('kv', None, 'tp'), may hold values from -6 to 6
- past_write: bfloat16 [256, 7, 1024], P('kv', None, 'tp'), may hold values from -6 to 6
- past_read: bfloat16 [256, 7, 1024], P('kv', None, 'tp'), may hold values from -6 to 6
- past_step: bfloat16 [256, 4, 64], P('kv', None, 'tp'), may hold values from -4 to 4
- accepted: int32 [256], P('kv'), may hold values from 1 to 4
Outputs:
- mixed: bfloat16 [256, 4, 2048], P('kv', None, 'tp')
- root_state: float32 [256, 64, 64, 128], P('kv', 'tp')
- next_value: bfloat16 [256, 7, 4096], P('kv', None, 'tp')
- next_write: bfloat16 [256, 7, 1024], P('kv', None, 'tp')
- next_read: bfloat16 [256, 7, 1024], P('kv', None, 'tp')
- next_step: bfloat16 [256, 4, 64], P('kv', None, 'tp')
Inputs may be any that keep to these rules, and one draw needn't show every extreme that they name: Every entry of `accepted` is an integer from 1 to 4 (at least one of the last step's proposals is always accepted).
All inputs are finite; a program needn't handle non-finite values.
Results may differ from a plain program's by a relative error of at most 0.018.
Values may be sent and summed in bfloat16 or wider, within the bound.
A program may use at most 64 MiB of HBM per device.

v0:
```python
import jax
import jax.numpy as jnp
from jax import lax
from jax.sharding import PartitionSpec as P

STATE_DIM = 128
CONV_W = 4
EPSILON = 1e-06


def sent_together(arrays, axis, dim, along):
    ends, at = ([], 0)
    for a in arrays[:-1]:
        at += a.shape[along]
        ends.append(at)
    both = jnp.concatenate(arrays, axis=along)
    return tuple(jnp.split(lax.all_gather(both, axis, axis=dim, tiled=True), ends, axis=along))


def split_up(value, dim, peers):
    before, after = (value.shape[:dim], value.shape[dim + 1 :])
    return jnp.moveaxis(value.reshape(*before, peers, -1, *after), dim, 0)


def summed_on_arrival(value, axis, dim):
    pieces = split_up(value, dim, lax.axis_size(axis))
    arrived = lax.all_to_all(pieces, axis, split_axis=0, concat_axis=0, tiled=True)
    return arrived.astype(jnp.float32).sum(axis=0)


def causal_conv(rows, kernel):
    width = kernel.shape[0]
    count = rows.shape[0] - width + 1
    total = kernel[0] * rows[0:count]
    for offset in range(1, width):
        total = total + kernel[offset] * rows[offset : offset + count]
    return total


def advance(
    past_x,
    past_b,
    past_c,
    past_dt,
    taken,
    state_zero,
    value_now,
    write_now,
    read_now,
    gate_now,
    step_now,
    conv_value,
    conv_write,
    conv_read,
    step_bias,
    decay_log,
    skip_gain,
    output_gain,
):
    highest = lax.Precision.HIGHEST
    proposals = value_now.shape[0]
    head_count = step_bias.shape[0]
    group_count = write_now.shape[1] // STATE_DIM
    per_group = head_count // group_count
    head_width = value_now.shape[1] // head_count
    rate = jnp.exp(decay_log)
    prev_x = jax.nn.silu(causal_conv(past_x.astype(jnp.float32), conv_value)).reshape(
        proposals, head_count, head_width
    )
    prev_b = jax.nn.silu(causal_conv(past_b.astype(jnp.float32), conv_write)).reshape(
        proposals, group_count, STATE_DIM
    )
    prev_b = jnp.repeat(prev_b, per_group, axis=1)
    prev_dt = jax.nn.softplus(past_dt.astype(jnp.float32) + step_bias)
    live = (jnp.arange(proposals, dtype=jnp.int32) < taken)[:, None]
    prev_log = jnp.where(live, -rate * prev_dt, jnp.zeros_like(prev_dt))
    total_log = jnp.sum(prev_log, axis=0)
    tail_log = total_log - jnp.cumsum(prev_log, axis=0)
    weight_now = jnp.where(live, jnp.exp(tail_log) * prev_dt, jnp.zeros_like(prev_dt))
    root = jnp.exp(total_log)[:, None, None] * state_zero + jnp.einsum(
        "sh,shp,shn->hpn", weight_now, prev_x, prev_b, precision=highest
    )
    window_x = jnp.concatenate(
        [lax.dynamic_slice_in_dim(past_x, taken, CONV_W - 1, 0), value_now], axis=0
    )
    window_b = jnp.concatenate(
        [lax.dynamic_slice_in_dim(past_b, taken, CONV_W - 1, 0), write_now], axis=0
    )
    window_c = jnp.concatenate(
        [lax.dynamic_slice_in_dim(past_c, taken, CONV_W - 1, 0), read_now], axis=0
    )
    cur_x = jax.nn.silu(causal_conv(window_x.astype(jnp.float32), conv_value)).reshape(
        proposals, head_count, head_width
    )
    cur_b = jax.nn.silu(causal_conv(window_b.astype(jnp.float32), conv_write)).reshape(
        proposals, group_count, STATE_DIM
    )
    cur_c = jax.nn.silu(causal_conv(window_c.astype(jnp.float32), conv_read)).reshape(
        proposals, group_count, STATE_DIM
    )
    cur_b = jnp.repeat(cur_b, per_group, axis=1)
    cur_c = jnp.repeat(cur_c, per_group, axis=1)
    cur_dt = jax.nn.softplus(step_now.astype(jnp.float32) + step_bias)
    logs = jnp.cumsum(-rate * cur_dt, axis=0)
    carried = jnp.einsum("thn,hpn->thp", cur_c, root, precision=highest) * jnp.exp(logs)[:, :, None]
    lower = (jnp.arange(proposals)[:, None] >= jnp.arange(proposals)[None, :])[:, :, None]
    diff = logs[:, None, :] - logs[None, :, :]
    decay = jnp.where(
        lower, jnp.exp(jnp.where(lower, diff, jnp.zeros_like(diff))), jnp.zeros_like(diff)
    )
    scores = (
        jnp.einsum("thn,shn->tsh", cur_c, cur_b, precision=highest) * decay * cur_dt[None, :, :]
    )
    inner = jnp.einsum("tsh,shp->thp", scores, cur_x, precision=highest)
    mixed = carried + inner + skip_gain[None, :, None] * cur_x
    gated = mixed.reshape(proposals, -1) * jax.nn.silu(gate_now.astype(jnp.float32))
    grouped = gated.reshape(proposals, group_count, -1)
    grouped = grouped * lax.rsqrt(jnp.mean(grouped * grouped, axis=-1, keepdims=True) + EPSILON)
    result = (grouped.reshape(proposals, -1) * output_gain).astype(jnp.bfloat16)
    return (result, root, window_x, window_b, window_c)


def on_device(
    tokens,
    input_gain,
    gate_weight,
    value_weight,
    write_weight,
    read_weight,
    step_weight,
    conv_value,
    conv_write,
    conv_read,
    step_bias,
    decay_log,
    skip_gain,
    output_gain,
    out_weight,
    base_state,
    past_value,
    past_write,
    past_read,
    past_step,
    accepted,
):
    whole = lax.all_gather(tokens, "tp", axis=2, tiled=True)
    seq_local, proposals, width = whole.shape
    rows = whole.astype(jnp.float32)
    normed = (
        rows * lax.rsqrt(jnp.mean(rows * rows, axis=-1, keepdims=True) + EPSILON) * input_gain
    ).astype(jnp.bfloat16)
    flat = normed.reshape(seq_local * proposals, width)
    token_count = flat.shape[0]
    head_count = step_bias.shape[0]
    own_step = lax.dynamic_slice_in_dim(
        step_weight, lax.axis_index("tp") * head_count, head_count, 1
    )
    step_now = jnp.dot(flat, own_step, preferred_element_type=jnp.float32).astype(jnp.bfloat16)
    pieces = sent_together((gate_weight, value_weight, write_weight, read_weight), "kv", 0, 1)
    gate_sum, value_sum, write_sum, read_sum = tuple(
        (jnp.dot(flat, piece, preferred_element_type=jnp.float32) for piece in pieces)
    )
    gate_now = gate_sum.astype(jnp.bfloat16)
    value_now = value_sum.astype(jnp.bfloat16)
    write_now = write_sum.astype(jnp.bfloat16)
    read_now = read_sum.astype(jnp.bfloat16)
    shaped = [
        item.reshape(seq_local, proposals, item.shape[1])
        for item in (value_now, write_now, read_now, gate_now, step_now)
    ]
    stepper = jax.vmap(advance, in_axes=(0,) * 11 + (None,) * 7)
    normal_out, root_state, next_value, next_write, next_read = stepper(
        past_value,
        past_write,
        past_read,
        past_step,
        accepted,
        base_state,
        shaped[0],
        shaped[1],
        shaped[2],
        shaped[3],
        shaped[4],
        conv_value,
        conv_write,
        conv_read,
        step_bias,
        decay_log,
        skip_gain,
        output_gain,
    )
    flat_y = normal_out.reshape(token_count, -1)
    partial_sum = jnp.dot(
        flat_y,
        lax.all_gather(out_weight, "kv", axis=1, tiled=True),
        preferred_element_type=jnp.float32,
    )
    summed = summed_on_arrival(partial_sum.astype(jnp.bfloat16), "tp", 1)
    mixed = summed.astype(jnp.bfloat16).reshape(seq_local, proposals, summed.shape[1])
    return (mixed, root_state, next_value, next_write, next_read, shaped[4])


def solution(mesh):
    return jax.shard_map(
        on_device,
        mesh=mesh,
        in_specs=(
            P("kv", None, "tp"),
            P(),
            P("kv", "tp"),
            P("kv", "tp"),
            P("kv", "tp"),
            P("kv", "tp"),
            P(),
            P(None, "tp"),
            P(None, "tp"),
            P(None, "tp"),
            P("tp"),
            P("tp"),
            P("tp"),
            P("tp"),
            P("tp", "kv"),
            P("kv", "tp", None, None),
            P("kv", None, "tp"),
            P("kv", None, "tp"),
            P("kv", None, "tp"),
            P("kv", None, "tp"),
            P("kv"),
        ),
        out_specs=(
            P("kv", None, "tp"),
            P("kv", "tp", None, None),
            P("kv", None, "tp"),
            P("kv", None, "tp"),
            P("kv", None, "tp"),
            P("kv", None, "tp"),
        ),
        check_vma=False,
    )
```

profile of v0, /device:TPU:1, one launch (start us, length us, event | category | flops | bytes accessed | tf_op | source)
XLA Modules:
  0.0 207.6 jit_solution(918326364809412777)
XLA Ops:
  7.2 0.0 copy-start
  7.2 0.0 copy-start.2
  7.2 0.0 all-gather.3.cloned.1.call-start
  7.2 1.5 pad_maximum_fusion
  8.8 0.0 all-gather.3.cloned.1.call-update
  8.8 0.0 all-gather.5.cloned.1.call-start
  8.9 0.7 all-gather.5.cloned.1.call-update
  9.6 0.7 fusion.52
  10.2 0.7 iota_compare_fusion.1
  11.0 0.7 convert_element_type.70
  11.7 1.3 gather_fusion.2
  13.0 1.4 gather_fusion.1
  14.3 0.8 convert_element_type.69
  15.1 18.1 %all_gather.9 = bf16[4,4,2048]{2,1,0:T(4,128)(2,1)S(1)} all-gather(bf16[4,4,256]{2,1,0:T(4,128)(2,1)} %param.21), channel_id=1, replica_groups=mesh['kv'=64,'tp'=8] {'tp'}, dimensions={2}, use_global_device_ids=true | all-gather | bytes 73728 | tf_op jit(solution)/shard_map/all_gather | solution.py:146
  33.2 0.1 fusion.17
  33.3 0.8 fusion.19
  34.1 0.0 copy-done
  34.1 0.1 convolution_convert_fusion.3
  34.3 0.1 copy.86
  34.4 0.0 copy-start.4
  34.4 0.7 exponential_negate_fusion
  35.0 0.8 fusion.56
  35.9 0.1 copy.91
  36.0 1.3 gather_fusion
  37.3 0.8 slice_bitcast_fusion.7
  38.2 0.8 multiply_select_fusion
  39.0 0.1 copy.80
  39.1 0.1 copy.93
  39.2 0.8 slice_bitcast_fusion.3
  40.0 0.9 fusion.57
  40.9 0.0 copy-start.8
  40.9 60.4 %all-gather.3.cloned.1.call-done = bf16[2048,1280]{1,0:T(8,128)(2,1)} async-done(((bf16[32,1280]{1,0:T(8,128)(2,1)}), bf16[2048,1280]{1,0:T(8,128)(2,1)}) %all-gather.3.cloned.1.call-update) | async-done | bytes 5242896 | tf_op jit(solution)/shard_map/all_gather | solution.py:17
  101.3 1.2 convolution_convert_fusion.2
  102.5 0.0 copy-start.7
  102.5 1.2 convolution_convert_fusion.1
  103.8 0.0 copy-start.5
  103.8 0.0 copy-start.6
  103.9 2.0 fusion.6
  105.9 0.0 copy-start.3
  105.9 0.1 divide_multiply_fusion.1
  106.0 0.1 reshape.160
  106.2 0.1 reshape.167
  106.3 2.0 fusion.12
  108.2 0.1 reshape.173
  108.3 0.4 fusion.5
  108.7 0.4 fusion.21
  109.1 0.0 copy-done.2
  109.1 1.9 convolution_add_fusion
  111.0 0.0 copy-start.1
  111.1 1.7 fusion.34
  112.8 0.0 copy-done.4
  112.8 0.0 copy-done.8
  112.8 0.2 multiply_reduce_fusion
  113.0 0.1 reshape.170
  113.1 0.1 rsqrt.21
  113.2 70.7 %all-gather.5.cloned.1.call-done = bf16[512,2048]{0,1:T(8,128)(2,1)} async-done(((bf16[512,32]{0,1:T(8,128)(2,1)}), bf16[512,2048]{0,1:T(8,128)(2,1)}) %all-gather.5.cloned.1.call-update) | async-done | bytes 2097168 | tf_op jit(solution)/shard_map/all_gather | solution.py:195
  183.9 0.0 copy-done.7
  183.9 2.2 %convolution_convert_fusion = bf16[16,2048]{1,0:T(8,128)(2,1)S(1)} fusion(bf16[512,2048]{0,1:T(8,128)(2,1)} %all-gather.5.cloned.1.call-done, f32[16,512]{1,0:T(8,128)S(1)} %reshape.170, f32[16,512]{1,0:T(8,128)S(1)} %fusion.12, f32[512]{0:T(512)S(1)} %copy-done.7, f32[16]{0:T(128)S(1)} %rsqrt.21), kind=kOutput, calls=%fused_computation.3 | convolution fusion | flops 33652736 | bytes 2230336 | tf_op jit(solution)/shard_map/dot_general | solution.py:193
  186.1 0.0 copy-done.5
  186.1 0.0 copy-done.6
  186.2 13.9 %all_to_all.5 = bf16[8,16,256]{2,1,0:T(8,128)(2,1)S(1)} all-to-all(bf16[8,16,256]{2,1,0:T(8,128)(2,1)S(1)} %bitcast.67), channel_id=1, replica_groups=mesh['kv'=64,'tp'=8] {'tp'}, dimensions={0} | all-to-all | bytes 131072 | tf_op jit(solution)/shard_map/all_to_all | solution.py:27
  200.1 0.6 reshape.172
  200.7 0.0 copy-done.3
  200.7 0.0 copy-done.1
  (25 shorter events, 0.3 us)
Async XLA Ops:
  7.2 27.0 %copy-start = (bf16[2048,64]{0,1:T(8,128)(2,1)S(1)}, bf16[2048,64]{0,1:T(8,128)(2,1)}, u32[]{:S(2)}) copy-start(bf16[2048,64]{0,1:T(8,128)(2,1)} %param.27) | copy-start | bytes 786436
  7.2 101.9 %copy-start.2 = (f32[4,8,64,128]{3,2,1,0:T(8,128)S(1)}, f32[4,8,64,128]{3,2,1,0:T(8,128)}, u32[]{:S(2)}) copy-start(f32[4,8,64,128]{3,2,1,0:T(8,128)} %param.36) | copy-start | bytes 3145732
  7.2 94.1 %all-gather.3.cloned.1.call-start = ((), (), s32[]{:S(2)}) async-start(), calls=%async_computation.1 | async-start | bytes 5324800 | tf_op jit(solution)/shard_map/all_gather | solution.py:17
  8.8 175.1 %all-gather.5.cloned.1.call-start = ((), (), s32[]{:S(2)}) async-start(), calls=%async_computation.2 | async-start | bytes 2129920 | tf_op jit(solution)/shard_map/all_gather | solution.py:195
  34.4 78.4 %copy-start.4 = (bf16[16,8]{1,0:T(8,128)(2,1)}, bf16[16,8]{1,0:T(8,128)(2,1)S(1)}, u32[]{:S(2)}) copy-start(bf16[16,8]{1,0:T(8,128)(2,1)S(1)} %copy.86) | copy-start | bytes 772
  40.9 71.9 %copy-start.8 = (f32[8]{0:T(128)S(1)}, f32[8]{0:T(128)}, u32[]{:S(2)}) copy-start(f32[8]{0:T(128)} %param.33) | copy-start | bytes 100
  102.5 81.4 %copy-start.7 = (f32[512]{0:T(512)S(1)}, f32[512]{0:T(512)}, u32[]{:S(2)}) copy-start(f32[512]{0:T(512)} %param.34) | copy-start | bytes 6148
  103.8 82.4 %copy-start.5 = (bf16[4,7,128]{2,0,1:T(4,128)(2,1)}, bf16[4,7,128]{2,0,1:T(4,128)(2,1)S(1)}, u32[]{:S(2)}) copy-start(bf16[4,7,128]{2,0,1:T(4,128)(2,1)S(1)} %get-tuple-element.30) | copy-start | bytes 21508
  103.8 82.4 %copy-start.6 = (bf16[4,7,128]{2,0,1:T(4,128)(2,1)}, bf16[4,7,128]{2,0,1:T(4,128)(2,1)S(1)}, u32[]{:S(2)}) copy-start(bf16[4,7,128]{2,0,1:T(4,128)(2,1)S(1)} %get-tuple-element.31) | copy-start | bytes 21508
  105.9 94.8 %copy-start.3 = (bf16[4,7,512]{2,0,1:T(4,128)(2,1)}, bf16[4,7,512]{2,0,1:T(4,128)(2,1)S(1)}, u32[]{:S(2)}) copy-start(bf16[4,7,512]{2,0,1:T(4,128)(2,1)S(1)} %copy_dynamic-update-slice_fusion) | copy-start | bytes 86020
  111.0 89.7 %copy-start.1 = (f32[4,8,64,128]{3,2,1,0:T(8,128)}, f32[4,8,64,128]{3,2,1,0:T(8,128)S(1)}, u32[]{:S(2)}) copy-start(f32[4,8,64,128]{3,2,1,0:T(8,128)S(1)} %convolution_add_fusion) | copy-start | bytes 3145732
Sparse Core Ops, SparseCore 0:
  11.6 89.6 all-gather.2
  104.4 79.4 all-gather.4
where the time goes:
time: 208 us
  waiting for transfers between devices  132 us (63%)
  blocking collectives  32 us (15%)
  between operations  14.3 us (7%)
  matrix products  13.2 us (6%)
  local copies, waits for them, and re-layouts  8.14 us (4%)
  other arithmetic  8.01 us (4%)
    all_gather x1, waiting for transfers between devices, on_device(): lax.all_gather(out_weight, 'kv', axis=1, tiled=True)  70.7 us
    all_gather x1, waiting for transfers between devices, sent_together(): lax.all_gather(both, axis, axis=dim, tiled=True)  60.4 us
    all_gather x1, blocking collectives, on_device(): whole = lax.all_gather(tokens, 'tp', axis=2, tiled=True)  18.1 us
    all_to_all x1, blocking collectives, summed_on_arrival(): lax.all_to_all(pieces, axis, split_axis=0, concat_axis=0, tiled=True)  13.9 us
    dot_general x4, matrix products, on_device(): jnp.dot(flat, piece, preferred_element_type=jnp.float32)  6.38 us
  transfers between devices with their start and end apart: 2, of which 2 were waited for; matrix products, arithmetic and copies ran while one was open for 12% of the time, Pallas kernels for 0%

commit v1 on v0

--- a/solution.py
+++ b/solution.py
@@ -143,7 +143,12 @@
     past_step,
     accepted,
 ):
-    whole = lax.all_gather(tokens, "tp", axis=2, tiled=True)
+    ring = [tokens]
+    for hop in range(7):
+        ring.append(lax.ppermute(ring[-1], "tp", [(dev, (dev + 1) % 8) for dev in range(8)]))
+    whole = jnp.roll(
+        jnp.concatenate(ring[::-1], axis=2), (lax.axis_index("tp") + 1) * ring[0].shape[2], axis=2
+    )
     seq_local, proposals, width = whole.shape
     rows = whole.astype(jnp.float32)
     normed = (

time: 208 us -> 208 us (level)
  blocking collectives: 32 us -> 13.9 us
  waiting for transfers between devices: 132 us -> 146 us
  starting transfers between devices: 0.08 us -> 2.7 us
    ppermute x0 -> x7, waiting for transfers between devices: none -> 20.7 us  [on_device(): lax.ppermute(ring[-1], 'tp', [(dev, (dev + 1) % 8) for dev in range(8)])]
    all_gather x1 -> x0, blocking collectives: 18.1 us -> none  [on_device(): whole = lax.all_gather(tokens, 'tp', axis=2, tiled=True)]
    all_gather x1, waiting for transfers between devices: 60.4 us -> 54.1 us  [sent_together(): lax.all_gather(both, axis, axis=dim, tiled=True)]
    ppermute x0 -> x7, starting transfers between devices: none -> 2.62 us  [on_device(): lax.ppermute(ring[-1], 'tp', [(dev, (dev + 1) % 8) for dev in range(8)])]
  transfers between devices with their start and end apart: 2 -> 9, of which waited for: 2 -> 9; matrix products, arithmetic and copies ran while one was open for 12% -> 13% of each run, Pallas kernels for 0% -> 0%
where the time goes in v1:
time: 208 us
  waiting for transfers between devices  146 us (70%)
  between operations  14.4 us (7%)
  blocking collectives  13.9 us (7%)
  matrix products  13.2 us (6%)
  local copies, waits for them, and re-layouts  9.73 us (5%)
  other arithmetic  8.01 us (4%)
  starting transfers between devices  2.7 us (1%)
    all_gather x1, waiting for transfers between devices, on_device(): lax.all_gather(out_weight, 'kv', axis=1, tiled=True)  70.7 us
    all_gather x1, waiting for transfers between devices, sent_together(): lax.all_gather(both, axis, axis=dim, tiled=True)  54.1 us
    ppermute x7, waiting for transfers between devices, on_device(): lax.ppermute(ring[-1], 'tp', [(dev, (dev + 1) % 8) for dev in range(8)])  20.7 us
    all_to_all x1, blocking collectives, summed_on_arrival(): lax.all_to_all(pieces, axis, split_axis=0, concat_axis=0, tiled=True)  13.9 us
    dot_general x4, matrix products, on_device(): jnp.dot(flat, piece, preferred_element_type=jnp.float32)  6.4 us
  transfers between devices with their start and end apart: 9, of which 9 were waited for; matrix products, arithmetic and copies ran while one was open for 13% of the time, Pallas kernels for 0%

profile of v1, /device:TPU:1, one launch (start us, length us, event | category | flops | bytes accessed | tf_op | source)
XLA Modules:
  0.0 207.5 jit_solution(10378763679432191898)
XLA Ops:
  7.2 0.0 copy-start
  7.2 0.0 all-gather.3.cloned.1.call-start
  7.2 1.5 pad_maximum_fusion
  8.8 0.0 all-gather.3.cloned.1.call-update
  8.8 0.0 all-gather.5.cloned.1.call-start
  8.9 2.6 %collective-permute-start = (bf16[4,4,256]{2,1,0:T(4,128)(2,1)}, bf16[4,4,256]{2,1,0:T(4,128)(2,1)S(1)}, u32[]{:S(2)}, u32[]{:S(2)}) collective-permute-start(bf16[4,4,256]{2,1,0:T(4,128)(2,1)} %param.21), channel_id=1, source_target_pairs={{0,1},{1,2},{2,3},{3,4},{4,5},{5,6},{6,7},{7,0},{8,9},{9,10},{10,1... | collective-permute-start | bytes 24584 | tf_op jit(solution)/shard_map/ppermute | solution.py:148
  11.5 0.0 all-gather.5.cloned.1.call-update
  11.5 0.8 slice_bitcast_fusion.7
  12.3 0.9 fusion.57
  13.2 0.8 slice_bitcast_fusion.3
  14.0 0.7 iota_compare_fusion.1
  14.7 1.9 collective-permute-done
  16.6 0.7 fusion.52
  17.3 3.6 %collective-permute-done.1 = bf16[4,4,256]{2,1,0:T(4,128)(2,1)S(1)} collective-permute-done((bf16[4,4,256]{2,1,0:T(4,128)(2,1)S(1)}, bf16[4,4,256]{2,1,0:T(4,128)(2,1)S(1)}, u32[]{:S(2)}, u32[]{:S(2)}) %collective-permute-start.1) | collective-permute-done | bytes 8224 | tf_op jit(solution)/shard_map/ppermute | solution.py:148
  20.9 0.0 collective-permute-start.2
  20.9 0.7 exponential_negate_fusion
  21.5 1.4 gather_fusion.1
  22.9 2.2 %collective-permute-done.2 = bf16[4,4,256]{2,1,0:T(4,128)(2,1)S(1)} collective-permute-done((bf16[4,4,256]{2,1,0:T(4,128)(2,1)S(1)}, bf16[4,4,256]{2,1,0:T(4,128)(2,1)S(1)}, u32[]{:S(2)}, u32[]{:S(2)}) %collective-permute-start.2) | collective-permute-done | bytes 8224 | tf_op jit(solution)/shard_map/ppermute | solution.py:148
  25.2 0.0 collective-permute-start.3
  25.2 1.3 gather_fusion
  26.5 3.0 %collective-permute-done.3 = bf16[4,4,256]{2,1,0:T(4,128)(2,1)S(1)} collective-permute-done((bf16[4,4,256]{2,1,0:T(4,128)(2,1)S(1)}, bf16[4,4,256]{2,1,0:T(4,128)(2,1)S(1)}, u32[]{:S(2)}, u32[]{:S(2)}) %collective-permute-start.3) | collective-permute-done | bytes 8224 | tf_op jit(solution)/shard_map/ppermute | solution.py:148
  29.5 1.3 gather_fusion.2
  30.8 3.0 %collective-permute-done.4 = bf16[4,4,256]{2,1,0:T(4,128)(2,1)S(1)} collective-permute-done((bf16[4,4,256]{2,1,0:T(4,128)(2,1)S(1)}, bf16[4,4,256]{2,1,0:T(4,128)(2,1)S(1)}, u32[]{:S(2)}, u32[]{:S(2)}) %collective-permute-start.4) | collective-permute-done | bytes 8224 | tf_op jit(solution)/shard_map/ppermute | solution.py:148
  33.7 4.3 %collective-permute-done.5 = bf16[4,4,256]{2,1,0:T(4,128)(2,1)S(1)} collective-permute-done((bf16[4,4,256]{2,1,0:T(4,128)(2,1)S(1)}, bf16[4,4,256]{2,1,0:T(4,128)(2,1)S(1)}, u32[]{:S(2)}, u32[]{:S(2)}) %collective-permute-start.5) | collective-permute-done | bytes 8224 | tf_op jit(solution)/shard_map/ppermute | solution.py:148
  38.0 0.7 convert_element_type.70
  38.7 0.8 convert_element_type.69
  39.5 2.8 %collective-permute-done.6 = bf16[4,4,256]{2,1,0:T(4,128)(2,1)S(1)} collective-permute-done((bf16[4,4,256]{2,1,0:T(4,128)(2,1)S(1)}, bf16[4,4,256]{2,1,0:T(4,128)(2,1)S(1)}, u32[]{:S(2)}, u32[]{:S(2)}) %collective-permute-start.6) | collective-permute-done | bytes 8224 | tf_op jit(solution)/shard_map/ppermute | solution.py:148
  42.4 0.7 constant_dynamic-update-slice_fusion.8
  43.2 0.7 constant_dynamic-update-slice_fusion
  43.9 0.1 fusion.17
  44.1 0.8 fusion.19
  44.9 0.1 convolution_convert_fusion.3
  45.1 0.1 copy.86
  45.1 0.8 fusion.56
  46.0 0.1 copy.91
  46.1 0.8 multiply_select_fusion
  46.9 0.1 copy.80
  47.0 0.1 copy.93
  47.1 54.1 %all-gather.3.cloned.1.call-done = bf16[2048,1280]{1,0:T(8,128)(2,1)} async-done(((bf16[32,1280]{1,0:T(8,128)(2,1)}), bf16[2048,1280]{1,0:T(8,128)(2,1)}) %all-gather.3.cloned.1.call-update) | async-done | bytes 5242896 | tf_op jit(solution)/shard_map/all_gather | solution.py:17
  101.3 1.2 convolution_convert_fusion.2
  102.5 0.0 copy-start.7
  102.5 1.2 convolution_convert_fusion.1
  103.8 0.0 copy-start.5
  103.8 0.0 copy-start.6
  103.9 2.0 fusion.6
  105.9 0.0 copy-start.3
  105.9 0.1 divide_multiply_fusion.1
  106.0 0.1 reshape.160
  106.1 0.1 reshape.167
  106.2 2.0 fusion.12
  108.2 0.1 reshape.173
  108.3 0.4 fusion.5
  108.7 0.4 fusion.21
  109.1 1.9 convolution_add_fusion
  111.0 0.0 copy-start.1
  111.0 1.7 fusion.34
  112.8 0.2 multiply_reduce_fusion
  113.0 0.1 reshape.170
  113.1 0.1 rsqrt.21
  113.1 70.7 %all-gather.5.cloned.1.call-done = bf16[512,2048]{0,1:T(8,128)(2,1)} async-done(((bf16[512,32]{0,1:T(8,128)(2,1)}), bf16[512,2048]{0,1:T(8,128)(2,1)}) %all-gather.5.cloned.1.call-update) | async-done | bytes 2097168 | tf_op jit(solution)/shard_map/all_gather | solution.py:200
  183.9 2.2 %convolution_convert_fusion = bf16[16,2048]{1,0:T(8,128)(2,1)S(1)} fusion(bf16[512,2048]{0,1:T(8,128)(2,1)} %all-gather.5.cloned.1.call-done, f32[16,512]{1,0:T(8,128)S(1)} %reshape.170, f32[16,512]{1,0:T(8,128)S(1)} %fusion.12, f32[512]{0:T(512)S(1)} %copy-done.7, f32[16]{0:T(128)S(1)} %rsqrt.21), kind=kOutput, calls=%fused_computation.3 | convolution fusion | flops 33652736 | bytes 2230336 | tf_op jit(solution)/shard_map/dot_general | solution.py:198
  186.1 0.0 copy-done.6
  186.1 13.9 %all_to_all.5 = bf16[8,16,256]{2,1,0:T(8,128)(2,1)S(1)} all-to-all(bf16[8,16,256]{2,1,0:T(8,128)(2,1)S(1)} %bitcast.67), channel_id=1, replica_groups=mesh['kv'=64,'tp'=8] {'tp'}, dimensions={0} | all-to-all | bytes 131072 | tf_op jit(solution)/shard_map/all_to_all | solution.py:27
  200.1 0.6 reshape.172
  (54 shorter events, 0.5 us)
Async XLA Ops:
  7.2 37.7 %copy-start = (bf16[2048,64]{0,1:T(8,128)(2,1)S(1)}, bf16[2048,64]{0,1:T(8,128)(2,1)}, u32[]{:S(2)}) copy-start(bf16[2048,64]{0,1:T(8,128)(2,1)} %param.27) | copy-start | bytes 786436
  7.2 101.9 %copy-start.2 = (f32[4,8,64,128]{3,2,1,0:T(8,128)S(1)}, f32[4,8,64,128]{3,2,1,0:T(8,128)}, u32[]{:S(2)}) copy-start(f32[4,8,64,128]{3,2,1,0:T(8,128)} %param.36) | copy-start | bytes 3145732
  7.2 94.1 %all-gather.3.cloned.1.call-start = ((), (), s32[]{:S(2)}) async-start(), calls=%async_computation.1 | async-start | bytes 5324800 | tf_op jit(solution)/shard_map/all_gather | solution.py:17
  8.8 175.0 %all-gather.5.cloned.1.call-start = ((), (), s32[]{:S(2)}) async-start(), calls=%async_computation.2 | async-start | bytes 2129920 | tf_op jit(solution)/shard_map/all_gather | solution.py:200
  8.9 7.7 %collective-permute-start = (bf16[4,4,256]{2,1,0:T(4,128)(2,1)}, bf16[4,4,256]{2,1,0:T(4,128)(2,1)S(1)}, u32[]{:S(2)}, u32[]{:S(2)}) collective-permute-start(bf16[4,4,256]{2,1,0:T(4,128)(2,1)} %param.21), channel_id=1, source_target_pairs={{0,1},{1,2},{2,3},{3,4},{4,5},{5,6},{6,7},{7,0},{8,9},{9,10},{10,1... | collective-permute-start | bytes 24584 | tf_op jit(solution)/shard_map/ppermute | solution.py:148
  16.6 4.3 %collective-permute-start.1 = (bf16[4,4,256]{2,1,0:T(4,128)(2,1)S(1)}, bf16[4,4,256]{2,1,0:T(4,128)(2,1)S(1)}, u32[]{:S(2)}, u32[]{:S(2)}) collective-permute-start(bf16[4,4,256]{2,1,0:T(4,128)(2,1)S(1)} %collective-permute-done), channel_id=1, source_target_pairs={{0,1},{1,2},{2,3},{3,4},{4,5},{5,6},{6,7},{7,0},{8,9},{9,10},{10,1... | collective-permute-start | bytes 24584 | tf_op jit(solution)/shard_map/ppermute | solution.py:148
  20.9 4.3 %collective-permute-start.2 = (bf16[4,4,256]{2,1,0:T(4,128)(2,1)S(1)}, bf16[4,4,256]{2,1,0:T(4,128)(2,1)S(1)}, u32[]{:S(2)}, u32[]{:S(2)}) collective-permute-start(bf16[4,4,256]{2,1,0:T(4,128)(2,1)S(1)} %collective-permute-done.1), channel_id=1, source_target_pairs={{0,1},{1,2},{2,3},{3,4},{4,5},{5,6},{6,7},{7,0},{8,9},{9,10},{10,1... | collective-permute-start | bytes 24584 | tf_op jit(solution)/shard_map/ppermute | solution.py:148
  25.2 4.3 %collective-permute-start.3 = (bf16[4,4,256]{2,1,0:T(4,128)(2,1)S(1)}, bf16[4,4,256]{2,1,0:T(4,128)(2,1)S(1)}, u32[]{:S(2)}, u32[]{:S(2)}) collective-permute-start(bf16[4,4,256]{2,1,0:T(4,128)(2,1)S(1)} %collective-permute-done.2), channel_id=1, source_target_pairs={{0,1},{1,2},{2,3},{3,4},{4,5},{5,6},{6,7},{7,0},{8,9},{9,10},{10,1... | collective-permute-start | bytes 24584 | tf_op jit(solution)/shard_map/ppermute | solution.py:148
  29.4 4.3 %collective-permute-start.4 = (bf16[4,4,256]{2,1,0:T(4,128)(2,1)S(1)}, bf16[4,4,256]{2,1,0:T(4,128)(2,1)S(1)}, u32[]{:S(2)}, u32[]{:S(2)}) collective-permute-start(bf16[4,4,256]{2,1,0:T(4,128)(2,1)S(1)} %collective-permute-done.3), channel_id=1, source_target_pairs={{0,1},{1,2},{2,3},{3,4},{4,5},{5,6},{6,7},{7,0},{8,9},{9,10},{10,1... | collective-permute-start | bytes 24584 | tf_op jit(solution)/shard_map/ppermute | solution.py:148
  33.7 4.3 %collective-permute-start.5 = (bf16[4,4,256]{2,1,0:T(4,128)(2,1)S(1)}, bf16[4,4,256]{2,1,0:T(4,128)(2,1)S(1)}, u32[]{:S(2)}, u32[]{:S(2)}) collective-permute-start(bf16[4,4,256]{2,1,0:T(4,128)(2,1)S(1)} %collective-permute-done.4), channel_id=1, source_target_pairs={{0,1},{1,2},{2,3},{3,4},{4,5},{5,6},{6,7},{7,0},{8,9},{9,10},{10,1... | collective-permute-start | bytes 24584 | tf_op jit(solution)/shard_map/ppermute | solution.py:148
  38.0 4.3 %collective-permute-start.6 = (bf16[4,4,256]{2,1,0:T(4,128)(2,1)S(1)}, bf16[4,4,256]{2,1,0:T(4,128)(2,1)S(1)}, u32[]{:S(2)}, u32[]{:S(2)}) collective-permute-start(bf16[4,4,256]{2,1,0:T(4,128)(2,1)S(1)} %collective-permute-done.5), channel_id=1, source_target_pairs={{0,1},{1,2},{2,3},{3,4},{4,5},{5,6},{6,7},{7,0},{8,9},{9,10},{10,1... | collective-permute-start | bytes 24584 | tf_op jit(solution)/shard_map/ppermute | solution.py:148
  45.1 67.6 %copy-start.4 = (bf16[16,8]{1,0:T(8,128)(2,1)}, bf16[16,8]{1,0:T(8,128)(2,1)S(1)}, u32[]{:S(2)}) copy-start(bf16[16,8]{1,0:T(8,128)(2,1)S(1)} %copy.86) | copy-start | bytes 772
  47.1 65.6 %copy-start.8 = (f32[8]{0:T(128)S(1)}, f32[8]{0:T(128)}, u32[]{:S(2)}) copy-start(f32[8]{0:T(128)} %param.33) | copy-start | bytes 100
  102.5 81.4 %copy-start.7 = (f32[512]{0:T(512)S(1)}, f32[512]{0:T(512)}, u32[]{:S(2)}) copy-start(f32[512]{0:T(512)} %param.34) | copy-start | bytes 6148
  103.8 82.3 %copy-start.5 = (bf16[4,7,128]{2,0,1:T(4,128)(2,1)}, bf16[4,7,128]{2,0,1:T(4,128)(2,1)S(1)}, u32[]{:S(2)}) copy-start(bf16[4,7,128]{2,0,1:T(4,128)(2,1)S(1)} %get-tuple-element.30) | copy-start | bytes 21508
  103.8 82.3 %copy-start.6 = (bf16[4,7,128]{2,0,1:T(4,128)(2,1)}, bf16[4,7,128]{2,0,1:T(4,128)(2,1)S(1)}, u32[]{:S(2)}) copy-start(bf16[4,7,128]{2,0,1:T(4,128)(2,1)S(1)} %get-tuple-element.31) | copy-start | bytes 21508
  105.9 94.8 %copy-start.3 = (bf16[4,7,512]{2,0,1:T(4,128)(2,1)}, bf16[4,7,512]{2,0,1:T(4,128)(2,1)S(1)}, u32[]{:S(2)}) copy-start(bf16[4,7,512]{2,0,1:T(4,128)(2,1)S(1)} %constant_dynamic-update-slice_fusion.18) | copy-start | bytes 86020
  111.0 89.6 %copy-start.1 = (f32[4,8,64,128]{3,2,1,0:T(8,128)}, f32[4,8,64,128]{3,2,1,0:T(8,128)S(1)}, u32[]{:S(2)}) copy-start(f32[4,8,64,128]{3,2,1,0:T(8,128)S(1)} %convolution_add_fusion) | copy-start | bytes 3145732
Sparse Core Ops, SparseCore 0:
  11.6 89.6 all-gather.2
  104.3 79.4 all-gather.4
